TPU v7x, 128 devices: a whole 4x4x4 slice. The times are simulated.
128 devices in a mesh: sp: 16 (over z, y), dp: 8 (over x, core).
Axes of the slice: x: 4, y: 4, z: 4, core: 2. Of those that a mesh axis runs over, the one named last changes fastest.
Arguments:
- u_pre: bfloat16 [8, 16384, 2048], P('dp', 'sp'), may hold values from -6 to 6
- v_pre: bfloat16 [8, 16384, 2048], P('dp', 'sp'), may hold values from -6 to 6
- d_out: bfloat16 [8, 16384, 2048], P('dp', 'sp'), may hold values from -6 to 6
- w_mix: bfloat16 [16, 128, 128], replicated, may hold values from -0.5 to 0.5
- mix_bias: float32 [16, 128], replicated, may hold values from 0.1 to 1.9
- norm_gain: float32 [16, 128], replicated, may hold values from 0.1 to 1.9
- norm_shift: float32 [16, 128], replicated, may hold values from -3 to 3
- w_out: bfloat16 [2048, 2048], P('dp'), may hold values from -0.125 to 0.125
Outputs:
- grad_u: bfloat16 [8, 16384, 2048], P('dp', 'sp')
- grad_v: bfloat16 [8, 16384, 2048], P('dp', 'sp')
- grad_w_out: float32 [2048, 2048], P('dp')
- grad_w_mix: float32 [16, 128, 128], replicated
- grad_mix_bias: float32 [16, 128], replicated
- grad_gain: float32 [16, 128], replicated
- grad_shift: float32 [16, 128], replicated
All inputs are finite; a program needn't handle non-finite values.
Results may differ from a plain program's by a relative error of at most 0.012.
Values may be sent and summed in bfloat16 or wider, within the bound.
A program may use at most 192 MiB of HBM per device.

v0:
```python
import jax
import jax.numpy as jnp
from jax import lax
from jax.sharding import PartitionSpec as P

EPS = 1e-05


def together(arrays, axis):
    ends = [0]
    for a in arrays:
        ends.append(ends[-1] + a.size)
    total = lax.psum(jnp.concatenate([a.ravel() for a in arrays]), axis)
    return tuple((total[b:e].reshape(a.shape) for a, b, e in zip(arrays, ends, ends[1:])))


def mechanism(grad_s, u_pre, v_pre, w_mix, mix_bias, gain, shift):
    items, length, width = grad_s.shape
    groups, span = (w_mix.shape[0], w_mix.shape[1])
    chans = width // groups
    shape = (items, length // span, span, groups, chans)
    u_val = u_pre.astype(jnp.float32).reshape(shape)
    v_val = v_pre.astype(jnp.float32).reshape(shape)
    cotan = grad_s.astype(jnp.float32).reshape(shape)
    upper, u_back = jax.vjp(jax.nn.gelu, u_val)
    gated, v_back = jax.vjp(jax.nn.gelu, v_val)
    centre = gated - jnp.mean(gated, axis=-1, keepdims=True)
    inverse = lax.rsqrt(jnp.mean(centre * centre, axis=-1, keepdims=True) + EPS)
    scaled = centre * inverse
    normed = (scaled * gain + shift).astype(jnp.bfloat16)
    lower = jnp.tril(jnp.ones((span, span), dtype=bool))
    w_low = jnp.where(lower[None], w_mix, jnp.zeros_like(w_mix))
    mixed = jnp.einsum("gts,insgc->intgc", w_low, normed, preferred_element_type=jnp.float32)
    mixed = mixed + jnp.transpose(mix_bias)[:, :, None]
    gated_out = (upper * mixed).astype(jnp.bfloat16)
    d_mixed = cotan * upper
    d_mixed_b = d_mixed.astype(jnp.bfloat16)
    grad_u = u_back(cotan * mixed)[0].astype(jnp.bfloat16).reshape(items, length, width)
    grad_bias = jnp.transpose(jnp.sum(d_mixed, axis=(0, 1, 4)))
    grad_w = jnp.einsum("intgc,insgc->gts", d_mixed_b, normed, preferred_element_type=jnp.float32)
    grad_w = jnp.where(lower[None], grad_w, jnp.zeros_like(grad_w))
    d_normed = jnp.einsum("gts,intgc->insgc", w_low, d_mixed_b, preferred_element_type=jnp.float32)
    grad_gain = jnp.sum(d_normed * scaled, axis=(0, 1, 2))
    grad_shift = jnp.sum(d_normed, axis=(0, 1, 2))
    d_scaled = d_normed * gain
    d_gated = inverse * (
        d_scaled
        - jnp.mean(d_scaled, axis=-1, keepdims=True)
        - scaled * jnp.mean(d_scaled * scaled, axis=-1, keepdims=True)
    )
    grad_v = v_back(d_gated)[0].astype(jnp.bfloat16).reshape(items, length, width)
    return (
        grad_u,
        grad_v,
        gated_out.reshape(items, length, width),
        grad_w,
        grad_bias,
        grad_gain,
        grad_shift,
    )


def on_device(u_pre, v_pre, d_out, w_mix, mix_bias, norm_gain, norm_shift, w_out):
    grad_s = lax.dot_general(
        d_out,
        lax.all_gather(w_out, "dp", axis=0, tiled=True),
        (((2,), (1,)), ((), ())),
        preferred_element_type=jnp.float32,
    ).astype(jnp.bfloat16)
    grad_u, grad_v, gated_out, grad_w, grad_bias, grad_gain, grad_shift = mechanism(
        grad_s, u_pre, v_pre, w_mix, mix_bias, norm_gain, norm_shift
    )
    grad_w, grad_bias, grad_gain, grad_shift = together(
        (grad_w, grad_bias, grad_gain, grad_shift), ("sp", "dp")
    )
    width = gated_out.shape[2]
    flat_d = d_out.reshape(-1, d_out.shape[2])
    flat_s = gated_out.reshape(-1, width)
    partial_rows = lax.psum_scatter(
        lax.dot_general(
            flat_s, flat_d, (((0,), (0,)), ((), ())), preferred_element_type=jnp.float32
        ),
        "dp",
        scatter_dimension=0,
        tiled=True,
    )
    grad_w_out = lax.psum(partial_rows, "sp")
    return (grad_u, grad_v, grad_w_out, grad_w, grad_bias, grad_gain, grad_shift)


def solution(mesh):
    return jax.shard_map(
        on_device,
        mesh=mesh,
        in_specs=(
            P("dp", "sp", None),
            P("dp", "sp", None),
            P("dp", "sp", None),
            P(),
            P(),
            P(),
            P(),
            P("dp", None),
        ),
        out_specs=(P("dp", "sp", None), P("dp", "sp", None), P("dp", None), P(), P(), P(), P()),
        check_vma=False,
    )
```

profile of v0, /device:TPU:0, one launch (start us, length us, event | category | flops | bytes accessed | tf_op | source)
XLA Modules:
  0.0 474.1 jit_solution(16673040196392679940)
XLA Ops:
  7.9 3.2 convert_bitcast_fusion
  11.2 5.2 %copy.67 = f32[128,8,16,128]{3,2,1,0:T(8,128)} copy(f32[128,8,16,128]{3,1,2,0:T(8,128)S(1)} %convert_bitcast_fusion) | data formatting | bytes 16777216
  16.4 9.1 %copy.45 = f32[1,8,128,16,128]{2,4,1,3,0:T(8,128)} copy(f32[1,8,128,16,128]{4,3,0,2,1:T(8,128)} %bitcast.100) | data formatting | bytes 16777216 | tf_op jit(solution)/shard_map/reshape | solution.py:22
  28.8 5.2 %copy.65 = f32[128,8,16,128]{3,2,1,0:T(8,128)} copy(f32[128,8,16,128]{3,1,2,0:T(8,128)S(1)} %convert_bitcast_fusion.1) | data formatting | bytes 16777216
  34.0 8.7 %copy.39 = f32[1,8,128,16,128]{2,4,1,3,0:T(8,128)} copy(f32[1,8,128,16,128]{4,3,0,2,1:T(8,128)} %bitcast.104) | data formatting | bytes 16777216 | tf_op jit(solution)/shard_map/reshape | solution.py:23
  42.8 5.9 %fusion.54 = f32[8,128,16]{1,0,2:T(8,128)S(1)} fusion(f32[1,8,128,16,128]{2,4,1,3,0:T(8,128)} %copy.39), kind=kLoop, calls=%fused_computation.83 | loop fusion | flops 18857984 | bytes 8454144 | tf_op jit(solution)/shard_map/reduce_sum | solution.py:27
  48.9 3.7 multiply_reduce_fusion.2
  52.7 6.5 %fusion.35 = bf16[8,128,16,128]{3,1,0,2:T(8,128)(2,1)} fusion(f32[8,128,16,128]{3,2,1,0:T(8,128)S(1)} %bitcast.105, f32[16,128]{1,0:T(8,128)S(1)} %copy-done.4, f32[16,128]{1,0:T(8,128)S(1)} %copy-done.3, f32[8,128,16]{1,0,2:T(8,128)S(1)} %add_rsqrt_fusion, f32[8,128,16]{1,0,2:T(8,128)S(1)} %broadcast_multiply_fusion.2), kind=kLoop, calls=%fused_computation.52 | loop fusion | flops 27262976 | bytes 12730368 | tf_op jit(solution)/shard_map/convert_element_type | solution.py:30
  61.8 13.1 %convert_bitcast_fusion.2 = f32[128,8,16,128]{3,1,2,0:T(8,128)S(1)} fusion(bf16[2048,2048]{1,0:T(8,128)(2,1)} %all-gather.2.cloned.1.call-done, bf16[1,1024,2048]{2,1,0:T(8,128)(2,1)} %param.10), kind=kOutput, calls=%fused_computation.51 | convolution fusion | flops 8594128896 | bytes 20971520 | tf_op jit(solution)/shard_map/dot_general | solution.py:64
  74.9 5.2 %copy.64 = f32[128,8,16,128]{3,2,1,0:T(8,128)} copy(f32[128,8,16,128]{3,1,2,0:T(8,128)S(1)} %convert_bitcast_fusion.2) | data formatting | bytes 16777216
  80.1 8.8 %copy.41 = f32[1,8,128,16,128]{2,4,1,3,0:T(8,128)} copy(f32[1,8,128,16,128]{4,3,2,1,0:T(8,128)} %bitcast.102) | data formatting | bytes 16777216 | tf_op jit(solution)/shard_map/reshape | solution.py:24
  88.9 14.8 %multiply_convert_fusion = (bf16[1,8,128,16,128]{2,4,1,3,0:T(8,128)(2,1)}, bf16[1,8,128,16,128]{2,4,1,3,0:T(8,128)(2,1)}, f32[128,16]{0,1:T(8,128)S(1)}) fusion(f32[128,16]{0,1:T(8,128)S(1)} %bitcast.112, f32[1,8,128,16,128]{2,4,1,3,0:T(8,128)} %copy.45, f32[1,8,128,16,128]{2,4,1,3,0:T(8,128)} %copy.41, bf16[8,128,16,128]{3,1,0,2:T(8,128)(2,1)} %fusion.35, ...), kind=kOutput, calls=%fused_computation.46 | convolution fusion | flops 593754112 | bytes 29917184 | tf_op jit(solution)/shard_map/gts,insgc->intgc/dot_general | solution.py:33
  103.7 6.8 %copy.58 = bf16[1,8,128,16,128]{4,3,2,1,0:T(8,128)(2,1)} copy(bf16[1,8,128,16,128]{2,4,1,3,0:T(8,128)(2,1)} %get-tuple-element.11) | data formatting | bytes 8388608 | tf_op jit(solution)/shard_map/convert_element_type | solution.py:35
  110.5 15.4 %fusion.37 = f32[2048,2048]{1,0:T(8,128)} fusion(bf16[128,8,16,128]{3,2,1,0:T(8,128)(2,1)} %bitcast.107, bf16[1,1024,2048]{2,1,0:T(8,128)(2,1)} %param.10), kind=kOutput, calls=%fused_computation.57 | convolution fusion | flops 8589934592 | bytes 25165824 | tf_op jit(solution)/shard_map/dot_general | solution.py:80
  125.9 10.2 %fusion.33 = bf16[8,128,16,128]{3,1,0,2:T(8,128)(2,1)S(1)} fusion(f32[8,128,16,128]{3,2,1,0:T(8,128)} %bitcast.103, f32[8,128,16,128]{3,2,1,0:T(8,128)} %bitcast.101), kind=kLoop, calls=%fused_computation.39 | loop fusion | flops 20971520 | bytes 20971520 | tf_op jit(solution)/shard_map/convert_element_type | solution.py:37
  137.4 10.3 %fusion.34 = (f32[16,128]{1,0:T(8,128)S(1)}, f32[8,128,16]{1,0,2:T(8,128)S(1)}, f32[8,128,16]{1,0,2:T(8,128)S(1)}, f32[16,128]{1,0:T(8,128)S(1)}, f32[16,8,128,128]{3,2,1,0:T(8,128)}) fusion(f32[8,128,16]{1,0,2:T(8,128)S(1)} %add_rsqrt_fusion, f32[8,128,16]{1,0,2:T(8,128)S(1)} %broadcast_multiply_fusion.2, f32[1,8,128,16,128]{2,4,1,3,0:T(8,128)} %copy.39, ...), kind=kOutput, calls=%fused_computation.44 | convolution fusion | flops 572747776 | bytes 21798912 | tf_op jit(solution)/shard_map/gts,intgc->insgc/dot_general | solution.py:42
  148.9 7.0 %copy.47 = bf16[1,8,128,16,128]{4,3,2,1,0:T(8,128)(2,1)} copy(bf16[1,8,128,16,128]{2,4,1,3,0:T(8,128)(2,1)} %get-tuple-element.12) | data formatting | bytes 8388608 | tf_op jit(solution)/shard_map/convert_element_type | solution.py:38
  155.8 7.3 %reshape.497 = bf16[1,1024,2048]{2,1,0:T(8,128)(2,1)} reshape(bf16[1,8,128,16,128]{4,3,2,1,0:T(8,128)(2,1)} %copy.47) | data formatting | bytes 8388608 | tf_op jit(solution)/shard_map/reshape | solution.py:38
  163.2 54.8 %reduce-scatter.2.cloned.1.call-done = f32[256,2048]{1,0:T(8,128)} async-done(((f32[2048,2048]{1,0:T(8,128)}), f32[256,2048]{1,0:T(8,128)}) %reduce-scatter.2.cloned.1.call-update) | async-done | bytes 2097168 | tf_op jit(solution)/shard_map/reduce_scatter | solution.py:79
  218.0 12.0 %fusion.6 = bf16[1,8,128,16,128]{2,4,1,3,0:T(8,128)(2,1)} fusion(f32[1,8,128,16,128]{2,4,1,3,0:T(8,128)} %copy.39, f32[16,8,128,128]{3,2,1,0:T(8,128)} %get-tuple-element.17, f32[8,128,16]{1,0,2:T(8,128)S(1)} %get-tuple-element.18, f32[8,128,16]{1,0,2:T(8,128)S(1)} %get-tuple-element.19, f32[16,128]{1,0:T(8,128)S(1)} %copy-done.3, ...), kind=kLoop, calls=%fused_computation.12 | loop fusion | flops 58720256 | bytes 21241856 | tf_op jit(solution)/shard_map/convert_element_type | solution.py:51
  230.0 6.7 %copy.56 = bf16[1,8,128,16,128]{4,3,2,1,0:T(8,128)(2,1)} copy(bf16[1,8,128,16,128]{2,4,1,3,0:T(8,128)(2,1)} %fusion.6) | data formatting | bytes 8388608 | tf_op jit(solution)/shard_map/convert_element_type | solution.py:51
  236.8 7.3 %reshape.500 = bf16[1,1024,2048]{2,1,0:T(8,128)(2,1)} reshape(bf16[1,8,128,16,128]{4,3,2,1,0:T(8,128)(2,1)} %copy.56) | data formatting | bytes 8388608 | tf_op jit(solution)/shard_map/reshape | solution.py:51
  244.1 127.2 %all-reduce.5.cloned.1.call-done = f32[268288]{0:T(1024)} async-done(((f32[268288]{0:T(1024)}), f32[268288]{0:T(1024)}) %all-reduce.5.cloned.1.call-update) | async-done | bytes 1073168 | tf_op jit(solution)/shard_map/psum | solution.py:13
  374.8 89.4 %all-reduce.3.cloned.1.call-done = f32[256,2048]{1,0:T(8,128)} async-done(((f32[256,2048]{1,0:T(8,128)}), f32[256,2048]{1,0:T(8,128)}) %all-reduce.3.cloned.1.call-update) | async-done | bytes 2097168 | tf_op jit(solution)/shard_map/psum | solution.py:87
  (33 shorter events, 16.2 us)
Async XLA Ops:
  7.2 54.7 %all-gather.2.cloned.1.call-start = ((), (), s32[]{:S(2)}) async-start(), calls=%async_computation.1 | async-start | bytes 9437184 | tf_op jit(solution)/shard_map/all_gather | solution.py:66
  7.9 210.1 %reduce-scatter.2.cloned.1.call-start = ((), (), s32[]{:S(2)}) async-start(), calls=%async_computation.2 | async-start | bytes 18874368 | tf_op jit(solution)/shard_map/reduce_scatter | solution.py:79
  42.7 6.2 %copy-start = (f32[1,8,128,16,128]{2,4,1,3,0:T(8,128)S(1)}, f32[1,8,128,16,128]{2,4,1,3,0:T(8,128)}, u32[]{:S(2)}) copy-start(f32[1,8,128,16,128]{2,4,1,3,0:T(8,128)} %copy.39) | copy-start | bytes 25165828
  42.7 9.9 %copy-start.1 = (f32[128,8,16,128]{3,2,1,0:T(8,128)S(1)}, f32[128,8,16,128]{3,2,1,0:T(8,128)}, u32[]{:S(2)}) copy-start(f32[128,8,16,128]{3,2,1,0:T(8,128)} %copy.65) | copy-start | bytes 25165828
  42.7 9.9 %copy-start.3 = (f32[16,128]{1,0:T(8,128)S(1)}, f32[16,128]{1,0:T(8,128)}, u32[]{:S(2)}) copy-start(f32[16,128]{1,0:T(8,128)} %param.13) | copy-start | bytes 24580
  42.7 9.9 %copy-start.4 = (f32[16,128]{1,0:T(8,128)S(1)}, f32[16,128]{1,0:T(8,128)}, u32[]{:S(2)}) copy-start(f32[16,128]{1,0:T(8,128)} %param.14) | copy-start | bytes 24580
  80.1 8.8 %copy-start.5 = (bf16[16,128,128]{2,1,0:T(8,128)(2,1)S(1)}, bf16[16,128,128]{2,1,0:T(8,128)(2,1)}, u32[]{:S(2)}) copy-start(bf16[16,128,128]{2,1,0:T(8,128)(2,1)} %param.11) | copy-start | bytes 1572868
  80.1 8.8 %copy-start.6 = (f32[16,128]{1,0:T(8,128)S(1)}, f32[16,128]{1,0:T(8,128)}, u32[]{:S(2)}) copy-start(f32[16,128]{1,0:T(8,128)} %param.12) | copy-start | bytes 24580
  125.9 245.4 %all-reduce.5.cloned.1.call-start = ((), (), s32[]{:S(2)}) async-start(), calls=%async_computation.4 | async-start | bytes 2146304 | tf_op jit(solution)/shard_map/psum | solution.py:13
  125.9 10.2 %copy-start.2 = (bf16[8,128,16,128]{3,1,0,2:T(8,128)(2,1)S(1)}, bf16[8,128,16,128]{3,1,0,2:T(8,128)(2,1)}, u32[]{:S(2)}) copy-start(bf16[8,128,16,128]{3,1,0,2:T(8,128)(2,1)} %fusion.35) | copy-start | bytes 12582916
  148.8 315.4 %all-reduce.3.cloned.1.call-start = ((), (), s32[]{:S(2)}) async-start(), calls=%async_computation.3 | async-start | bytes 4194304 | tf_op jit(solution)/shard_map/psum | solution.py:87
Sparse Core Ops, SparseCore 0:
  9.7 52.0 all-gather.1
  126.0 91.9 reduce-scatter.1
  223.3 147.8 all-reduce.4
  374.4 89.7 all-reduce.2
where the time goes:
time: 478 us; the launch traced here: 474 us
  waiting for transfers between devices  275 us (58%)
  local copies, waits for them, and re-layouts  84.4 us (18%)
  matrix products  54.8 us (11%)
  other arithmetic  45.8 us (10%)
  between operations  14.1 us (3%)
    psum x1, waiting for transfers between devices, together(): total = lax.psum(jnp.concatenate([a.ravel() for a in arrays]), axis)  127 us
    psum x1, waiting for transfers between devices, on_device(): grad_w_out = lax.psum(partial_rows, 'sp')  89.4 us
    reduce_scatter x1, waiting for transfers between devices, on_device(): lax.psum_scatter(lax.dot_general(flat_s, flat_d, (((0,), (0,)), ((), ()))...  54.8 us
    unnamed x18, local copies, waits for them, and re-layouts  19 us
    dot_general x1, matrix products, on_device(): lax.dot_general(flat_s, flat_d, (((0,), (0,)), ((), ())), preferred_eleme...  15.4 us
    dot_general x1, matrix products, mechanism(): jnp.einsum('gts,insgc->intgc', w_low, normed, preferred_element_type=jnp....  14.8 us
    dot_general x1, matrix products, on_device(): lax.dot_general(d_out, lax.all_gather(w_out, 'dp', axis=0, tiled=True), (...  13.1 us
    convert_element_type x1, other arithmetic, mechanism(): v_back(d_gated)[0].astype(jnp.bfloat16).reshape(items, length, width)  12 us
  transfers between devices with their start and end apart: 4, of which 4 were waited for; matrix products, arithmetic and copies ran while one was open for 25% of the time, Pallas kernels for 0%

commit v1 on v0

--- a/solution.py
+++ b/solution.py
@@ -84,7 +84,13 @@
         scatter_dimension=0,
         tiled=True,
     )
-    grad_w_out = lax.psum(partial_rows, "sp")
+    devices = lax.axis_size("sp")
+    grad_w_out, reach = (partial_rows, 1)
+    while reach < devices:
+        grad_w_out = grad_w_out + lax.ppermute(
+            grad_w_out, "sp", [(i, i ^ reach) for i in range(devices)]
+        )
+        reach = 2 * reach
     return (grad_u, grad_v, grad_w_out, grad_w, grad_bias, grad_gain, grad_shift)
 
 

time: 478 us -> 528 us (1.10)
  waiting for transfers between devices: 275 us -> 312 us
  starting transfers between devices: 0.16 us -> 9.64 us
  other arithmetic: 45.8 us -> 54.1 us
    ppermute x0 -> x4, waiting for transfers between devices: none -> 115 us  [on_device(): lax.ppermute(grad_w_out, 'sp', [(i, i ^ reach) for i in range(devices)])]
    psum x1 -> x0, waiting for transfers between devices: 89.4 us -> none  [on_device(): grad_w_out = lax.psum(partial_rows, 'sp')]
    reduce_scatter x1, waiting for transfers between devices: 54.8 us -> 92 us  [on_device(): lax.psum_scatter(lax.dot_general(flat_s, flat_d, (((0,), (0,)), ((), ()))...]
    psum x1, waiting for transfers between devices: 127 us -> 102 us  [together(): total = lax.psum(jnp.concatenate([a.ravel() for a in arrays]), axis)]
    ppermute x0 -> x4, starting transfers between devices: none -> 9.52 us  [on_device(): lax.ppermute(grad_w_out, 'sp', [(i, i ^ reach) for i in range(devices)])]
    add x0 -> x4, other arithmetic: none -> 7.96 us  [on_device(): grad_w_out + lax.ppermute(grad_w_out, 'sp', [(i, i ^ reach) for i in rang...]
    unnamed x18 -> x23, local copies, waits for them, and re-layouts: 19 us -> 15.8 us
  transfers between devices with their start and end apart: 4 -> 7, of which waited for: 4 -> 6; matrix products, arithmetic and copies ran while one was open for 25% -> 22% of each run, Pallas kernels for 0% -> 0%
where the time goes in v1:
time: 528 us; the launch traced here: 523 us
  waiting for transfers between devices  312 us (59%)
  local copies, waits for them, and re-layouts  80.8 us (15%)
  other arithmetic  54.1 us (10%)
  matrix products  52.5 us (10%)
  between operations  14.2 us (3%)
  starting transfers between devices  9.64 us (2%)
    ppermute x4, waiting for transfers between devices, on_device(): lax.ppermute(grad_w_out, 'sp', [(i, i ^ reach) for i in range(devices)])  115 us
    psum x1, waiting for transfers between devices, together(): total = lax.psum(jnp.concatenate([a.ravel() for a in arrays]), axis)  102 us
    reduce_scatter x1, waiting for transfers between devices, on_device(): lax.psum_scatter(lax.dot_general(flat_s, flat_d, (((0,), (0,)), ((), ()))...  92 us
    unnamed x23, local copies, waits for them, and re-layouts  15.8 us
    dot_general x1, matrix products, on_device(): lax.dot_general(flat_s, flat_d, (((0,), (0,)), ((), ())), preferred_eleme...  15.4 us
    dot_general x1, matrix products, mechanism(): jnp.einsum('gts,insgc->intgc', w_low, normed, preferred_element_type=jnp....  14.8 us
    dot_general x1, matrix products, on_device(): lax.dot_general(d_out, lax.all_gather(w_out, 'dp', axis=0, tiled=True), (...  13.1 us
    convert_element_type x1, other arithmetic, mechanism(): v_back(d_gated)[0].astype(jnp.bfloat16).reshape(items, length, width)  12.2 us
  transfers between devices with their start and end apart: 7, of which 6 were waited for; matrix products, arithmetic and copies ran while one was open for 22% of the time, Pallas kernels for 0%

profile of v1, /device:TPU:0, one launch (start us, length us, event | category | flops | bytes accessed | tf_op | source)
XLA Modules:
  0.0 523.4 jit_solution(356376718351816498)
XLA Ops:
  11.2 5.2 copy.67
  16.4 9.1 %copy.45 = f32[1,8,128,16,128]{2,4,1,3,0:T(8,128)} copy(f32[1,8,128,16,128]{4,3,0,2,1:T(8,128)} %bitcast.102) | data formatting | bytes 16777216 | tf_op jit(solution)/shard_map/reshape | solution.py:22
  28.7 5.2 copy.65
  33.9 8.7 %copy.39 = f32[1,8,128,16,128]{2,4,1,3,0:T(8,128)} copy(f32[1,8,128,16,128]{4,3,0,2,1:T(8,128)} %bitcast.106) | data formatting | bytes 16777216 | tf_op jit(solution)/shard_map/reshape | solution.py:23
  42.7 5.9 %fusion.54 = f32[8,128,16]{1,0,2:T(8,128)S(1)} fusion(f32[1,8,128,16,128]{2,4,1,3,0:T(8,128)} %copy.39), kind=kLoop, calls=%fused_computation.83 | loop fusion | flops 18857984 | bytes 8454144 | tf_op jit(solution)/shard_map/reduce_sum | solution.py:27
  52.6 6.5 %fusion.35 = bf16[8,128,16,128]{3,1,0,2:T(8,128)(2,1)} fusion(f32[8,128,16,128]{3,2,1,0:T(8,128)S(1)} %bitcast.107, f32[16,128]{1,0:T(8,128)S(1)} %copy-done.5, f32[16,128]{1,0:T(8,128)S(1)} %copy-done.4, f32[8,128,16]{1,0,2:T(8,128)S(1)} %add_rsqrt_fusion, f32[8,128,16]{1,0,2:T(8,128)S(1)} %broadcast_multiply_fusion.2), kind=kLoop, calls=%fused_computation.52 | loop fusion | flops 27262976 | bytes 12730368 | tf_op jit(solution)/shard_map/convert_element_type | solution.py:30
  61.8 13.1 %convert_bitcast_fusion.2 = f32[128,8,16,128]{3,1,2,0:T(8,128)S(1)} fusion(bf16[2048,2048]{1,0:T(8,128)(2,1)} %all-gather.2.cloned.1.call-done, bf16[1,1024,2048]{2,1,0:T(8,128)(2,1)} %param.10), kind=kOutput, calls=%fused_computation.51 | convolution fusion | flops 8594128896 | bytes 20971520 | tf_op jit(solution)/shard_map/dot_general | solution.py:64
  74.9 5.2 copy.64
  80.1 8.8 %copy.41 = f32[1,8,128,16,128]{2,4,1,3,0:T(8,128)} copy(f32[1,8,128,16,128]{4,3,2,1,0:T(8,128)} %bitcast.104) | data formatting | bytes 16777216 | tf_op jit(solution)/shard_map/reshape | solution.py:24
  88.9 14.8 %multiply_convert_fusion = (bf16[1,8,128,16,128]{2,4,1,3,0:T(8,128)(2,1)}, bf16[1,8,128,16,128]{2,4,1,3,0:T(8,128)(2,1)}, f32[128,16]{0,1:T(8,128)S(1)}) fusion(f32[128,16]{0,1:T(8,128)S(1)} %bitcast.114, f32[1,8,128,16,128]{2,4,1,3,0:T(8,128)} %copy.45, f32[1,8,128,16,128]{2,4,1,3,0:T(8,128)} %copy.41, bf16[8,128,16,128]{3,1,0,2:T(8,128)(2,1)} %fusion.35, ...), kind=kOutput, calls=%fused_computation.46 | convolution fusion | flops 593754112 | bytes 29917184 | tf_op jit(solution)/shard_map/gts,insgc->intgc/dot_general | solution.py:33
  103.7 6.8 %copy.58 = bf16[1,8,128,16,128]{4,3,2,1,0:T(8,128)(2,1)} copy(bf16[1,8,128,16,128]{2,4,1,3,0:T(8,128)(2,1)} %get-tuple-element.11) | data formatting | bytes 8388608 | tf_op jit(solution)/shard_map/convert_element_type | solution.py:35
  110.5 15.4 %fusion.37 = f32[2048,2048]{1,0:T(8,128)} fusion(bf16[128,8,16,128]{3,2,1,0:T(8,128)(2,1)} %bitcast.109, bf16[1,1024,2048]{2,1,0:T(8,128)(2,1)} %param.10), kind=kOutput, calls=%fused_computation.57 | convolution fusion | flops 8589934592 | bytes 25165824 | tf_op jit(solution)/shard_map/dot_general | solution.py:80
  125.9 92.0 %reduce-scatter.2.cloned.1.call-done = f32[256,2048]{1,0:T(8,128)} async-done(((f32[2048,2048]{1,0:T(8,128)}), f32[256,2048]{1,0:T(8,128)}) %reduce-scatter.2.cloned.1.call-update) | async-done | bytes 2097168 | tf_op jit(solution)/shard_map/reduce_scatter | solution.py:79
  219.5 45.6 %collective-permute-done = f32[256,2048]{1,0:T(8,128)S(1)} collective-permute-done((f32[256,2048]{1,0:T(8,128)}, f32[256,2048]{1,0:T(8,128)S(1)}, u32[]{:S(2)}, u32[]{:S(2)}) %collective-permute-start) | collective-permute-done | bytes 2097184 | tf_op jit(solution)/shard_map/ppermute | solution.py:90
  270.1 10.2 %fusion.33 = bf16[8,128,16,128]{3,1,0,2:T(8,128)(2,1)S(1)} fusion(f32[8,128,16,128]{3,2,1,0:T(8,128)} %bitcast.105, f32[8,128,16,128]{3,2,1,0:T(8,128)} %bitcast.103), kind=kLoop, calls=%fused_computation.39 | loop fusion | flops 20971520 | bytes 20971520 | tf_op jit(solution)/shard_map/convert_element_type | solution.py:37
  281.7 8.0 %fusion.34 = (f32[16,128]{1,0:T(8,128)S(1)}, f32[8,128,16]{1,0,2:T(8,128)S(1)}, f32[8,128,16]{1,0,2:T(8,128)S(1)}, f32[16,128]{1,0:T(8,128)S(1)}, f32[16,8,128,128]{3,2,1,0:T(8,128)}) fusion(f32[8,128,16]{1,0,2:T(8,128)S(1)} %add_rsqrt_fusion, f32[8,128,16]{1,0,2:T(8,128)S(1)} %broadcast_multiply_fusion.2, f32[1,8,128,16,128]{2,4,1,3,0:T(8,128)S(1)} %bitcast.101, ...), kind=kOutput, calls=%fused_computation.44 | convolution fusion | flops 572747776 | bytes 21798912 | tf_op jit(solution)/shard_map/gts,intgc->insgc/dot_general | solution.py:42
  289.7 25.0 %collective-permute-done.1 = f32[256,2048]{1,0:T(8,128)S(1)} collective-permute-done((f32[256,2048]{1,0:T(8,128)S(1)}, f32[256,2048]{1,0:T(8,128)S(1)}, u32[]{:S(2)}, u32[]{:S(2)}) %collective-permute-start.1) | collective-permute-done | bytes 2097184 | tf_op jit(solution)/shard_map/ppermute | solution.py:90
  318.0 44.5 %collective-permute-done.2 = f32[256,2048]{1,0:T(8,128)} collective-permute-done((f32[256,2048]{1,0:T(8,128)S(1)}, f32[256,2048]{1,0:T(8,128)}, u32[]{:S(2)}, u32[]{:S(2)}) %collective-permute-start.2) | collective-permute-done | bytes 2097184 | tf_op jit(solution)/shard_map/ppermute | solution.py:90
  368.1 12.2 %fusion.6 = bf16[1,8,128,16,128]{2,4,1,3,0:T(8,128)(2,1)} fusion(f32[1,8,128,16,128]{2,4,1,3,0:T(8,128)} %copy.39, f32[16,8,128,128]{3,2,1,0:T(8,128)} %get-tuple-element.17, f32[8,128,16]{1,0,2:T(8,128)S(1)} %get-tuple-element.18, f32[8,128,16]{1,0,2:T(8,128)S(1)} %get-tuple-element.19, f32[16,128]{1,0:T(8,128)S(1)} %copy-done.4, ...), kind=kLoop, calls=%fused_computation.12 | loop fusion | flops 58720256 | bytes 21241856 | tf_op jit(solution)/shard_map/convert_element_type | solution.py:51
  380.3 6.7 %copy.47 = bf16[1,8,128,16,128]{4,3,2,1,0:T(8,128)(2,1)} copy(bf16[1,8,128,16,128]{2,4,1,3,0:T(8,128)(2,1)} %get-tuple-element.12) | data formatting | bytes 8388608 | tf_op jit(solution)/shard_map/convert_element_type | solution.py:38
  387.0 7.3 %reshape.497 = bf16[1,1024,2048]{2,1,0:T(8,128)(2,1)} reshape(bf16[1,8,128,16,128]{4,3,2,1,0:T(8,128)(2,1)} %copy.47) | data formatting | bytes 8388608 | tf_op jit(solution)/shard_map/reshape | solution.py:38
  394.2 6.8 %copy.56 = bf16[1,8,128,16,128]{4,3,2,1,0:T(8,128)(2,1)} copy(bf16[1,8,128,16,128]{2,4,1,3,0:T(8,128)(2,1)} %fusion.6) | data formatting | bytes 8388608 | tf_op jit(solution)/shard_map/convert_element_type | solution.py:51
  401.0 7.3 %reshape.500 = bf16[1,1024,2048]{2,1,0:T(8,128)(2,1)} reshape(bf16[1,8,128,16,128]{4,3,2,1,0:T(8,128)(2,1)} %copy.56) | data formatting | bytes 8388608 | tf_op jit(solution)/shard_map/reshape | solution.py:51
  408.3 101.6 %all-reduce.2.cloned.1.call-done = f32[268288]{0:T(1024)} async-done(((f32[268288]{0:T(1024)}), f32[268288]{0:T(1024)}) %all-reduce.2.cloned.1.call-update) | async-done | bytes 1073168 | tf_op jit(solution)/shard_map/psum | solution.py:13
  (48 shorter events, 37.5 us)
Async XLA Ops:
  7.2 54.7 %all-gather.2.cloned.1.call-start = ((), (), s32[]{:S(2)}) async-start(), calls=%async_computation.1 | async-start | bytes 9437184 | tf_op jit(solution)/shard_map/all_gather | solution.py:66
  7.9 210.1 %reduce-scatter.2.cloned.1.call-start = ((), (), s32[]{:S(2)}) async-start(), calls=%async_computation.2 | async-start | bytes 18874368 | tf_op jit(solution)/shard_map/reduce_scatter | solution.py:79
  42.7 6.2 %copy-start = (f32[1,8,128,16,128]{2,4,1,3,0:T(8,128)S(1)}, f32[1,8,128,16,128]{2,4,1,3,0:T(8,128)}, u32[]{:S(2)}) copy-start(f32[1,8,128,16,128]{2,4,1,3,0:T(8,128)} %copy.39) | copy-start | bytes 25165828
  42.7 9.9 %copy-start.1 = (f32[128,8,16,128]{3,2,1,0:T(8,128)S(1)}, f32[128,8,16,128]{3,2,1,0:T(8,128)}, u32[]{:S(2)}) copy-start(f32[128,8,16,128]{3,2,1,0:T(8,128)} %copy.65) | copy-start | bytes 25165828
  42.7 9.9 %copy-start.4 = (f32[16,128]{1,0:T(8,128)S(1)}, f32[16,128]{1,0:T(8,128)}, u32[]{:S(2)}) copy-start(f32[16,128]{1,0:T(8,128)} %param.13) | copy-start | bytes 24580
  42.7 9.9 %copy-start.5 = (f32[16,128]{1,0:T(8,128)S(1)}, f32[16,128]{1,0:T(8,128)}, u32[]{:S(2)}) copy-start(f32[16,128]{1,0:T(8,128)} %param.14) | copy-start | bytes 24580
  80.1 8.8 %copy-start.6 = (bf16[16,128,128]{2,1,0:T(8,128)(2,1)S(1)}, bf16[16,128,128]{2,1,0:T(8,128)(2,1)}, u32[]{:S(2)}) copy-start(bf16[16,128,128]{2,1,0:T(8,128)(2,1)} %param.11) | copy-start | bytes 1572868
  80.1 8.8 %copy-start.7 = (f32[16,128]{1,0:T(8,128)S(1)}, f32[16,128]{1,0:T(8,128)}, u32[]{:S(2)}) copy-start(f32[16,128]{1,0:T(8,128)} %param.12) | copy-start | bytes 24580
  125.9 383.9 %all-reduce.2.cloned.1.call-start = ((), (), s32[]{:S(2)}) async-start(), calls=%async_computation.3 | async-start | bytes 2146304 | tf_op jit(solution)/shard_map/psum | solution.py:13
  218.0 47.1 %collective-permute-start = (f32[256,2048]{1,0:T(8,128)}, f32[256,2048]{1,0:T(8,128)S(1)}, u32[]{:S(2)}, u32[]{:S(2)}) collective-permute-start(f32[256,2048]{1,0:T(8,128)} %reduce-scatter.2.cloned.1.call-done), channel_id=1, source_target_pairs={{0,8},{8,0},{16,24},{24,16},{32,40},{40,32},{48,56},{56,48},{64,72... | collective-permute-start | bytes 6291464 | tf_op jit(solution)/shard_map/ppermute | solution.py:90
  265.0 16.6 %slice-start = ((s8[8388608]{0:T(1024)(128)(4,1)}), s8[4194304]{0:T(1024)(128)(4,1)S(1)}, s32[]{:S(2)}) async-start(s8[8388608]{0:T(1024)(128)(4,1)} %bitcast.100), calls=%async_computation.4 | async-start | bytes 8388608
  267.0 47.6 %collective-permute-start.1 = (f32[256,2048]{1,0:T(8,128)S(1)}, f32[256,2048]{1,0:T(8,128)S(1)}, u32[]{:S(2)}, u32[]{:S(2)}) collective-permute-start(f32[256,2048]{1,0:T(8,128)S(1)} %add.205), channel_id=1, source_target_pairs={{0,16},{8,24},{16,0},{24,8},{32,48},{40,56},{48,32},{56,40},{64,80... | collective-permute-start | bytes 6291464 | tf_op jit(solution)/shard_map/ppermute | solution.py:90
  270.1 10.2 %copy-start.2 = (bf16[8,128,16,128]{3,1,0,2:T(8,128)(2,1)S(1)}, bf16[8,128,16,128]{3,1,0,2:T(8,128)(2,1)}, u32[]{:S(2)}) copy-start(bf16[8,128,16,128]{3,1,0,2:T(8,128)(2,1)} %fusion.35) | copy-start | bytes 12582916
  270.1 11.5 %slice-start.1 = ((s8[8388608]{0:T(1024)(128)(4,1)}), s8[4194304]{0:T(1024)(128)(4,1)S(1)}, s32[]{:S(2)}) async-start(s8[8388608]{0:T(1024)(128)(4,1)} %bitcast.100), calls=%async_computation.5 | async-start | bytes 8388608
  315.0 3.0 copy-start.3
  315.0 47.6 %collective-permute-start.2 = (f32[256,2048]{1,0:T(8,128)S(1)}, f32[256,2048]{1,0:T(8,128)}, u32[]{:S(2)}, u32[]{:S(2)}) collective-permute-start(f32[256,2048]{1,0:T(8,128)S(1)} %add.206), channel_id=1, source_target_pairs={{0,32},{8,40},{16,48},{24,56},{32,0},{40,8},{48,16},{56,24},{64,96... | collective-permute-start | bytes 6291464 | tf_op jit(solution)/shard_map/ppermute | solution.py:90
  365.0 148.4 %collective-permute-start.3 = (f32[256,2048]{1,0:T(8,128)S(1)}, f32[256,2048]{1,0:T(8,128)}, u32[]{:S(2)}, u32[]{:S(2)}) collective-permute-start(f32[256,2048]{1,0:T(8,128)S(1)} %add.207), channel_id=1, source_target_pairs={{0,64},{8,72},{16,80},{24,88},{32,96},{40,104},{48,112},{56,120},{... | collective-permute-start | bytes 6291464 | tf_op jit(solution)/shard_map/ppermute | solution.py:90
Sparse Core Ops, SparseCore 0:
  9.7 52.0 all-gather.1
  126.0 91.9 reduce-scatter.1
  318.1 191.6 all-reduce.1
